TPU v7x, 32 devices: a whole 2x2x4 slice. The times are simulated.
32 devices in a mesh: fs: 4 (over y, x), tp: 8 (over z, core).
Axes of the slice: x: 2, y: 2, z: 4, core: 2. Of those that a mesh axis runs over, the one named last changes fastest.
Arguments:
- normed_inputs: bfloat16 [4096, 4096], P('fs', 'tp'), may hold values from -6 to 6
- query_upstream: bfloat16 [4096, 4096], P('fs', 'tp'), may hold values from -0.125 to 0.125
- key_upstream: bfloat16 [4096, 1024], P('fs', 'tp'), may hold values from -0.09375 to 0.09375
- head_outputs: bfloat16 [4096, 4096], P('fs', 'tp'), may hold values from -6 to 6
- branch_upstream: bfloat16 [4096, 4096], P('fs', 'tp'), may hold values from -0.125 to 0.125
- query_master: float32 [4096, 4096], P('fs', 'tp'), may hold values from -0.09375 to 0.09375
- key_master: float32 [4096, 1024], P('fs', 'tp'), may hold values from -0.09375 to 0.09375
- branch_master: float32 [4096, 4096], P('fs', 'tp'), may hold values from -0.09375 to 0.09375
- query_basis: bfloat16 [4096, 128], replicated, may hold values from -0.09375 to 0.09375
- key_basis: bfloat16 [4096, 128], replicated, may hold values from -0.09375 to 0.09375
- branch_basis: bfloat16 [4096, 128], replicated, may hold values from -0.09375 to 0.09375
- query_first: float32 [128, 4096], P(None, 'tp'), may hold values from -0.75 to 0.75
- query_second: float32 [128, 4096], P(None, 'tp'), may hold values from 0.001 to 0.02
- key_first: float32 [128, 1024], P(None, 'tp'), may hold values from -0.75 to 0.75
- key_second: float32 [128, 1024], P(None, 'tp'), may hold values from 0.001 to 0.02
- branch_first: float32 [4096, 128], P('fs'), may hold values from -0.75 to 0.75
- branch_second: float32 [4096, 128], P('fs'), may hold values from 0.001 to 0.02
Outputs:
- query_step: float32 [4096, 4096], P('fs', 'tp')
- key_step: float32 [4096, 1024], P('fs', 'tp')
- branch_step: float32 [4096, 4096], P('fs', 'tp')
- query_updated: float32 [4096, 4096], P('fs', 'tp')
- key_updated: float32 [4096, 1024], P('fs', 'tp')
- branch_updated: float32 [4096, 4096], P('fs', 'tp')
- query_copy: bfloat16 [4096, 4096], P(None, 'tp')
- key_copy: bfloat16 [4096, 1024], P(None, 'tp')
- branch_copy: bfloat16 [4096, 4096], P(None, 'tp')
- query_first_new: float32 [128, 4096], P(None, 'tp')
- query_second_new: float32 [128, 4096], P(None, 'tp')
- key_first_new: float32 [128, 1024], P(None, 'tp')
- key_second_new: float32 [128, 1024], P(None, 'tp')
- branch_first_new: float32 [4096, 128], P('fs')
- branch_second_new: float32 [4096, 128], P('fs')
All inputs are finite; a program needn't handle non-finite values.
Results may differ from a plain program's by a relative error of at most 0.001.
Values may be sent and summed in bfloat16 or wider, within the bound.
A program may use at most 128 MiB of HBM per device.

v0:
```python
import jax
import jax.numpy as jnp
from jax import lax
from jax.sharding import PartitionSpec as P

LEARN = 0.02
BETA_ONE = 0.9
BETA_TWO = 0.95
ADAM_EPS = 1e-08
CLIP_RMS = 0.5


def moments(first, second, low, clip):
    scaled = clip * low
    first_new = BETA_ONE * first + (1.0 - BETA_ONE) * scaled
    second_new = BETA_TWO * second + (1.0 - BETA_TWO) * scaled * scaled
    return (first_new, second_new, first_new / (jnp.sqrt(second_new) + ADAM_EPS))


def over_tokens(left, right, precision=None):
    return lax.dot_general(
        left,
        right,
        (((0,), (0,)), ((), ())),
        precision=precision,
        preferred_element_type=jnp.float32,
    )


def per_device(
    normed_inputs,
    query_upstream,
    key_upstream,
    head_outputs,
    branch_upstream,
    query_master,
    key_master,
    branch_master,
    query_basis,
    key_basis,
    branch_basis,
    query_first,
    query_second,
    key_first,
    key_second,
    branch_first,
    branch_second,
):
    exact = lax.Precision.HIGHEST
    row_index = lax.axis_index("fs")
    col_index = lax.axis_index("tp")
    n_rows = lax.axis_size("fs")
    n_cols = lax.axis_size("tp")
    features = normed_inputs.shape[1]
    query_local = query_upstream.shape[1]
    key_local = key_upstream.shape[1]
    rows_in = query_master.shape[0]
    rank = query_basis.shape[1]
    whole_values = lax.all_gather(head_outputs, "tp", axis=1, tiled=True)
    block_query = lax.dynamic_slice_in_dim(query_basis, col_index * features, features, 0)
    block_key = lax.dynamic_slice_in_dim(key_basis, col_index * features, features, 0)
    proj_query, proj_key = lax.psum(
        (
            jnp.dot(normed_inputs, block_query, preferred_element_type=jnp.float32),
            jnp.dot(normed_inputs, block_key, preferred_element_type=jnp.float32),
        ),
        "tp",
    )
    part_query = over_tokens(proj_query, query_upstream.astype(jnp.float32), exact)
    part_key = over_tokens(proj_key, key_upstream.astype(jnp.float32), exact)
    grad_branch = lax.psum_scatter(
        over_tokens(whole_values, branch_upstream), "fs", scatter_dimension=0, tiled=True
    )
    own_branch = lax.dynamic_slice_in_dim(branch_basis, col_index * features, features, 0).astype(
        jnp.float32
    )
    part_branch = jnp.dot(grad_branch, own_branch, precision=exact)
    query_low, key_low = lax.psum((part_query, part_key), "fs")
    branch_low = lax.psum(part_branch, "tp")
    local_squares = (jnp.sum(query_low * query_low) + jnp.sum(key_low * key_low)) / n_rows
    local_squares = local_squares + jnp.sum(branch_low * branch_low) / n_cols
    total = lax.psum(local_squares, ("fs", "tp"))
    entries = rank * n_cols * (2 * query_local + key_local)
    rms_value = jnp.sqrt(total / float(entries))
    clip = 1.0 / jnp.maximum(1.0, rms_value / CLIP_RMS)
    q_first, q_second, q_dir = moments(query_first, query_second, query_low, clip)
    k_first, k_second, k_dir = moments(key_first, key_second, key_low, clip)
    b_first, b_second, b_dir = moments(branch_first, branch_second, branch_low, clip)
    step_rows_query = lax.dynamic_slice_in_dim(query_basis, row_index * rows_in, rows_in, 0).astype(
        jnp.float32
    )
    step_rows_key = lax.dynamic_slice_in_dim(key_basis, row_index * rows_in, rows_in, 0).astype(
        jnp.float32
    )
    query_step = jnp.dot(step_rows_query, q_dir, precision=exact)
    key_step = jnp.dot(step_rows_key, k_dir, precision=exact)
    branch_step = jnp.dot(b_dir, own_branch.T, precision=exact)
    query_updated = query_master - LEARN * query_step
    key_updated = key_master - LEARN * key_step
    branch_updated = branch_master - LEARN * branch_step
    query_copy, key_copy, branch_copy = (
        lax.all_gather(query_updated.astype(jnp.bfloat16), "fs", axis=0, tiled=True),
        lax.all_gather(key_updated.astype(jnp.bfloat16), "fs", axis=0, tiled=True),
        lax.all_gather(branch_updated.astype(jnp.bfloat16), "fs", axis=0, tiled=True),
    )
    return (
        query_step,
        key_step,
        branch_step,
        query_updated,
        key_updated,
        branch_updated,
        query_copy,
        key_copy,
        branch_copy,
        q_first,
        q_second,
        k_first,
        k_second,
        b_first,
        b_second,
    )


def solution(mesh):
    return jax.shard_map(
        per_device,
        mesh=mesh,
        in_specs=(
            P("fs", "tp"),
            P("fs", "tp"),
            P("fs", "tp"),
            P("fs", "tp"),
            P("fs", "tp"),
            P("fs", "tp"),
            P("fs", "tp"),
            P("fs", "tp"),
            P(),
            P(),
            P(),
            P(None, "tp"),
            P(None, "tp"),
            P(None, "tp"),
            P(None, "tp"),
            P("fs", None),
            P("fs", None),
        ),
        out_specs=(
            P("fs", "tp"),
            P("fs", "tp"),
            P("fs", "tp"),
            P("fs", "tp"),
            P("fs", "tp"),
            P("fs", "tp"),
            P(None, "tp"),
            P(None, "tp"),
            P(None, "tp"),
            P(None, "tp"),
            P(None, "tp"),
            P(None, "tp"),
            P(None, "tp"),
            P("fs", None),
            P("fs", None),
        ),
        check_vma=False,
    )
```

profile of v0, /device:TPU:0, one launch (start us, length us, event | category | flops | bytes accessed | tf_op | source)
XLA Modules:
  0.0 502.3 jit_solution(1356573704103843505)
XLA Ops:
  7.2 0.7 all-gather.5.cloned.1.call-update
  8.0 86.4 %all-gather.5.cloned.1.call-done = bf16[1024,4096]{1,0:T(8,128)(2,1)} async-done(((bf16[1024,512]{1,0:T(8,128)(2,1)}), bf16[1024,4096]{1,0:T(8,128)(2,1)}) %all-gather.5.cloned.1.call-update) | async-done | bytes 8388624 | tf_op jit(solution)/shard_map/all_gather | solution.py:59
  94.4 10.4 %fusion.39 = f32[4096,512]{1,0:T(8,128)} fusion(bf16[1024,4096]{1,0:T(8,128)(2,1)} %all-gather.5.cloned.1.call-done, bf16[1024,512]{1,0:T(8,128)(2,1)S(1)} %copy-done), kind=kOutput, calls=%fused_computation.53 | convolution fusion | flops 4294967296 | bytes 17825792 | tf_op jit(solution)/shard_map/dot_general | solution.py:21
  104.9 0.0 all-reduce.5.cloned.1.call-start
  104.9 1.1 copy-done.2
  106.1 2.2 convolution_bitcast_fusion
  108.2 2.2 convolution_bitcast_fusion.1
  110.4 79.4 %reduce-scatter.2.cloned.1.call-done = f32[1024,512]{1,0:T(8,128)} async-done(((f32[4096,512]{1,0:T(8,128)}), f32[1024,512]{1,0:T(8,128)}) %reduce-scatter.2.cloned.1.call-update) | async-done | bytes 2097168 | tf_op jit(solution)/shard_map/reduce_scatter | solution.py:71
  189.8 3.4 fusion.18
  193.4 62.4 %all-reduce.5.cloned.1.call-done = (f32[1024,128]{0,1:T(8,128)}, f32[1024,128]{0,1:T(8,128)}, f32[1024,128]{1,0:T(8,128)}) async-done(((f32[1024,128]{0,1:T(8,128)}, f32[1024,128]{0,1:T(8,128)}, f32[1024,128]{1,0:T(8,128)}), (f32[1024,128]{0,1:T(8,128)}, f32[1024,128]{0,1:T(8,128)}, f32[1024,128]{1,0:T(8,128)})) %all-reduce.5.cloned.1.call-update) | async-done | bytes 1572880 | tf_op jit(solution)/shard_map/psum | solution.py:62
  255.8 2.5 fusion.37
  258.3 1.0 fusion.38
  259.3 0.0 all-gather.9.cloned.1.call-start
  259.4 0.7 multiply_reduce_fusion
  260.7 41.6 %all-reduce.7.cloned.1.call-done = (f32[128,512]{1,0:T(8,128)}, f32[128,128]{1,0:T(8,128)}) async-done(((f32[128,512]{1,0:T(8,128)}, f32[128,128]{1,0:T(8,128)}), (f32[128,512]{1,0:T(8,128)}, f32[128,128]{1,0:T(8,128)})) %all-reduce.7.cloned.1.call-update) | async-done | bytes 327696 | tf_op jit(solution)/shard_map/psum | solution.py:78
  302.3 1.6 multiply_reduce_fusion.1
  303.9 1.5 multiply_reduce_fusion.2
  306.7 39.3 %psum.47 = f32[]{:T(128)} all-reduce(f32[]{:T(128)S(6)} %add.68), channel_id=1, replica_groups=mesh['fs'=4,'tp'=8] {'fs','tp'}, use_global_device_ids=true, to_apply=%region_9.0 | all-reduce | flops 1 | bytes 8 | tf_op jit(solution)/shard_map/psum | solution.py:82
  346.8 0.9 fusion.20
  347.7 2.6 fusion.35
  350.3 0.0 all-gather.11.cloned.1.call-start
  350.3 1.4 fusion
  351.7 4.7 fusion.34
  356.5 1.2 fusion.5
  357.7 0.4 copy-done.8
  358.1 4.5 fusion.36
  362.7 15.2 %all-gather.9.cloned.1.call-done = bf16[4096,128]{1,0:T(8,128)(2,1)} async-done(((bf16[1024,128]{1,0:T(8,128)(2,1)}), bf16[4096,128]{1,0:T(8,128)(2,1)}) %all-gather.9.cloned.1.call-update) | async-done | bytes 1048592 | tf_op jit(solution)/shard_map/all_gather | solution.py:103
  377.9 54.9 %all-gather.11.cloned.1.call-done = bf16[4096,512]{1,0:T(8,128)(2,1)} async-done(((bf16[1024,512]{1,0:T(8,128)(2,1)}), bf16[4096,512]{1,0:T(8,128)(2,1)}) %all-gather.11.cloned.1.call-update) | async-done | bytes 4194320 | tf_op jit(solution)/shard_map/all_gather | solution.py:104
  432.8 55.0 %all-gather.7.cloned.1.call-done = bf16[4096,512]{1,0:T(8,128)(2,1)} async-done(((bf16[1024,512]{1,0:T(8,128)(2,1)}), bf16[4096,512]{1,0:T(8,128)(2,1)}) %all-gather.7.cloned.1.call-update) | async-done | bytes 4194320 | tf_op jit(solution)/shard_map/all_gather | solution.py:102
  487.8 4.6 copy.40
  492.5 1.0 copy.41
  493.4 2.0 copy.42
  (52 shorter events, 0.4 us)
Async XLA Ops:
  7.2 87.2 %copy-start = (bf16[1024,512]{1,0:T(8,128)(2,1)S(1)}, bf16[1024,512]{1,0:T(8,128)(2,1)}, u32[]{:S(2)}) copy-start(bf16[1024,512]{1,0:T(8,128)(2,1)} %param.21) | copy-start | bytes 3145732
  7.2 87.2 %all-gather.5.cloned.1.call-start = ((), (), s32[]{:S(2)}) async-start(), calls=%async_computation.1 | async-start | bytes 9437184 | tf_op jit(solution)/shard_map/all_gather | solution.py:59
  7.9 181.9 %reduce-scatter.2.cloned.1.call-start = ((), (), s32[]{:S(2)}) async-start(), calls=%async_computation.2 | async-start | bytes 10485760 | tf_op jit(solution)/shard_map/reduce_scatter | solution.py:71
  104.9 1.2 copy-start.2
  104.9 150.9 %all-reduce.5.cloned.1.call-start = ((), (), s32[]{:S(2)}) async-start(), calls=%async_computation.6 | async-start | bytes 3145728 | tf_op jit(solution)/shard_map/psum | solution.py:62
  110.4 145.4 %copy-start.11 = (bf16[1024,512]{1,0:T(8,128)(2,1)S(1)}, bf16[1024,512]{1,0:T(8,128)(2,1)}, u32[]{:S(2)}) copy-start(bf16[1024,512]{1,0:T(8,128)(2,1)} %param.18) | copy-start | bytes 3145732
  193.3 65.0 %copy-start.19 = (bf16[1024,128]{1,0:T(8,128)(2,1)S(1)}, bf16[1024,128]{1,0:T(8,128)(2,1)}, u32[]{:S(2)}) copy-start(bf16[1024,128]{1,0:T(8,128)(2,1)} %param.19) | copy-start | bytes 786436
  193.3 153.5 %copy-start.20 = (f32[128,128]{1,0:T(8,128)S(1)}, f32[128,128]{1,0:T(8,128)}, u32[]{:S(2)}) copy-start(f32[128,128]{1,0:T(8,128)} %param.31) | copy-start | bytes 196612
  193.3 153.5 %copy-start.21 = (f32[128,128]{1,0:T(8,128)S(1)}, f32[128,128]{1,0:T(8,128)}, u32[]{:S(2)}) copy-start(f32[128,128]{1,0:T(8,128)} %param.30) | copy-start | bytes 196612
  193.3 109.0 %all-reduce.7.cloned.1.call-start = ((), (), s32[]{:S(2)}) async-start(), calls=%async_computation.7 | async-start | bytes 655360 | tf_op jit(solution)/shard_map/psum | solution.py:78
  255.8 2.5 copy-start.15
  255.8 3.6 copy-start.6
  255.8 91.9 %copy-start.14 = (f32[1024,128]{1,0:T(8,128)S(1)}, f32[1024,128]{1,0:T(8,128)}, u32[]{:S(2)}) copy-start(f32[1024,128]{1,0:T(8,128)} %param.23) | copy-start | bytes 1572868
  259.3 118.6 %all-gather.9.cloned.1.call-start = ((), (), s32[]{:S(2)}) async-start(), calls=%async_computation.4 | async-start | bytes 1310720 | tf_op jit(solution)/shard_map/all_gather | solution.py:103
  347.6 4.0 copy-start.17
  347.6 4.0 copy-start.18
  347.7 4.0 copy-start.7
  350.3 82.5 %all-gather.11.cloned.1.call-start = ((), (), s32[]{:S(2)}) async-start(), calls=%async_computation.5 | async-start | bytes 5242880 | tf_op jit(solution)/shard_map/all_gather | solution.py:104
  351.7 4.7 copy-start.4
  351.7 4.7 copy-start.5
  351.7 4.8 copy-start.12
  351.7 4.8 copy-start.16
  356.4 1.7 copy-start.8
  356.4 131.4 %all-gather.7.cloned.1.call-start = ((), (), s32[]{:S(2)}) async-start(), calls=%async_computation.3 | async-start | bytes 5242880 | tf_op jit(solution)/shard_map/all_gather | solution.py:102
  357.7 5.0 copy-start.9
  357.7 5.0 copy-start.10
  487.8 4.6 copy-start.13
  487.8 5.6 %copy-start.3 = (bf16[4096,512]{1,0:T(8,128)(2,1)S(1)}, bf16[4096,512]{1,0:T(8,128)(2,1)}, u32[]{:S(2)}) copy-start(bf16[4096,512]{1,0:T(8,128)(2,1)} %all-gather.11.cloned.1.call-done) | copy-start | bytes 12582916
  493.4 2.0 copy-start.1
Sparse Core Ops, SparseCore 0:
  9.6 84.7 all-gather.4
  105.0 84.7 reduce-scatter.1
  193.6 62.1 all-reduce.4
  259.4 42.8 all-reduce.6
  350.4 27.4 all-gather.8
  380.2 52.5 all-gather.10
  435.2 52.5 all-gather.6
where the time goes:
time: 503 us; the launch traced here: 502 us
  waiting for transfers between devices  396 us (79%)
  blocking collectives  39.3 us (8%)
  matrix products  33.4 us (7%)
  between operations  17 us (3%)
  local copies, waits for them, and re-layouts  9.28 us (2%)
  other arithmetic  7.2 us (1%)
    all_gather x1, waiting for transfers between devices, per_device(): whole_values = lax.all_gather(head_outputs, 'tp', axis=1, tiled=True)  86.4 us
    reduce_scatter x1, waiting for transfers between devices, per_device(): lax.psum_scatter(over_tokens(whole_values, branch_upstream), 'fs', scatte...  79.4 us
    psum x1, waiting for transfers between devices, per_device(): lax.psum((jnp.dot(normed_inputs, block_query, preferred_element_type=jnp....  62.4 us
    all_gather x1, waiting for transfers between devices, per_device(): lax.all_gather(query_updated.astype(jnp.bfloat16), 'fs', axis=0, tiled=True)  55 us
    all_gather x1, waiting for transfers between devices, per_device(): lax.all_gather(branch_updated.astype(jnp.bfloat16), 'fs', axis=0, tiled=T...  54.9 us
    psum x1, waiting for transfers between devices, per_device(): query_low, key_low = lax.psum((part_query, part_key), 'fs')  41.6 us
    psum x1, blocking collectives, per_device(): total = lax.psum(local_squares, ('fs', 'tp'))  39.3 us
    all_gather x1, waiting for transfers between devices, per_device(): lax.all_gather(key_updated.astype(jnp.bfloat16), 'fs', axis=0, tiled=True)  15.2 us
  transfers between devices with their start and end apart: 7, of which 7 were waited for; matrix products, arithmetic and copies ran while one was open for 3% of the time, Pallas kernels for 0%

commit v1 on v0

--- a/solution.py
+++ b/solution.py
@@ -56,30 +56,35 @@
     key_local = key_upstream.shape[1]
     rows_in = query_master.shape[0]
     rank = query_basis.shape[1]
-    whole_values = lax.all_gather(head_outputs, "tp", axis=1, tiled=True)
-    block_query = lax.dynamic_slice_in_dim(query_basis, col_index * features, features, 0)
-    block_key = lax.dynamic_slice_in_dim(key_basis, col_index * features, features, 0)
-    proj_query, proj_key = lax.psum(
+    def own_block(basis):
+        return lax.dynamic_slice_in_dim(basis, col_index * features, features, 0)
+
+    block_branch = own_block(branch_basis)
+    proj_query, proj_key, proj_branch = lax.psum(
         (
-            jnp.dot(normed_inputs, block_query, preferred_element_type=jnp.float32),
-            jnp.dot(normed_inputs, block_key, preferred_element_type=jnp.float32),
+            jnp.dot(normed_inputs, own_block(query_basis), preferred_element_type=jnp.float32),
+            jnp.dot(normed_inputs, own_block(key_basis), preferred_element_type=jnp.float32),
+            jnp.dot(branch_upstream, block_branch, preferred_element_type=jnp.float32),
         ),
         "tp",
     )
     part_query = over_tokens(proj_query, query_upstream.astype(jnp.float32), exact)
     part_key = over_tokens(proj_key, key_upstream.astype(jnp.float32), exact)
-    grad_branch = lax.psum_scatter(
-        over_tokens(whole_values, branch_upstream), "fs", scatter_dimension=0, tiled=True
+    part_branch = over_tokens(head_outputs.astype(jnp.float32), proj_branch, exact)
+    own_branch = block_branch.astype(jnp.float32)
+    query_low, key_low, branch_block = lax.psum((part_query, part_key, part_branch), "fs")
+    local_squares = (
+        jnp.sum(query_low * query_low)
+        + jnp.sum(key_low * key_low)
+        + jnp.sum(branch_block * branch_block)
     )
-    own_branch = lax.dynamic_slice_in_dim(branch_basis, col_index * features, features, 0).astype(
-        jnp.float32
-    )
-    part_branch = jnp.dot(grad_branch, own_branch, precision=exact)
-    query_low, key_low = lax.psum((part_query, part_key), "fs")
-    branch_low = lax.psum(part_branch, "tp")
-    local_squares = (jnp.sum(query_low * query_low) + jnp.sum(key_low * key_low)) / n_rows
-    local_squares = local_squares + jnp.sum(branch_low * branch_low) / n_cols
-    total = lax.psum(local_squares, ("fs", "tp"))
+    rows_block = branch_block.shape[0]
+    carried = jnp.concatenate([branch_block, jnp.full((8, rank), local_squares)], axis=0)
+    gathered = lax.all_gather(carried, "tp", axis=0)
+    total = jnp.sum(gathered[:, rows_block, 0])
+    branch_all = gathered[:, :rows_block, :].reshape(n_cols * rows_block, rank)
+    own_rows = branch_first.shape[0]
+    branch_low = lax.dynamic_slice_in_dim(branch_all, row_index * own_rows, own_rows, 0)
     entries = rank * n_cols * (2 * query_local + key_local)
     rms_value = jnp.sqrt(total / float(entries))
     clip = 1.0 / jnp.maximum(1.0, rms_value / CLIP_RMS)

time: 503 us -> 324 us (0.64)
  waiting for transfers between devices: 396 us -> 264 us
  blocking collectives: 39.3 us -> 0 us
  matrix products: 33.4 us -> 21.6 us
    reduce_scatter x1 -> x0, waiting for transfers between devices: 79.4 us -> none  [per_device(): lax.psum_scatter(over_tokens(whole_values, branch_upstream), 'fs', scatte...]
    all_gather x1, waiting for transfers between devices: 86.4 us -> 29.5 us  [per_device(): gathered = lax.all_gather(carried, 'tp', axis=0)]
    psum x1 -> x0, blocking collectives: 39.3 us -> none  [per_device(): total = lax.psum(local_squares, ('fs', 'tp'))]
    dot_general x3, matrix products: 13.9 us -> 4.75 us  [over_tokens(): lax.dot_general(left, right, (((0,), (0,)), ((), ())), precision=precisio...]
    psum x2, waiting for transfers between devices: 104 us -> 111 us  [the longest x1 65 us: per_device(): lax.psum((jnp.dot(normed_inputs, own_block(query_basis), preferred_elemen...]
    unnamed x47 -> x46, local copies, waits for them, and re-layouts: 9.28 us -> 10.9 us
  transfers between devices with their start and end apart: 7 -> 6, of which waited for: 7 -> 6; matrix products, arithmetic and copies ran while one was open for 3% -> 3% of each run, Pallas kernels for 0% -> 0%
where the time goes in v1:
time: 324 us; the launch traced here: 323 us
  waiting for transfers between devices  264 us (81%)
  matrix products  21.6 us (7%)
  between operations  17 us (5%)
  local copies, waits for them, and re-layouts  11.7 us (4%)
  other arithmetic  8.68 us (3%)
    psum x1, waiting for transfers between devices, per_device(): lax.psum((jnp.dot(normed_inputs, own_block(query_basis), preferred_elemen...  65 us
    all_gather x1, waiting for transfers between devices, per_device(): lax.all_gather(query_updated.astype(jnp.bfloat16), 'fs', axis=0, tiled=True)  54.9 us
    all_gather x1, waiting for transfers between devices, per_device(): lax.all_gather(branch_updated.astype(jnp.bfloat16), 'fs', axis=0, tiled=T...  54.9 us
    psum x1, waiting for transfers between devices, per_device(): lax.psum((part_query, part_key, part_branch), 'fs')  45.7 us
    all_gather x1, waiting for transfers between devices, per_device(): gathered = lax.all_gather(carried, 'tp', axis=0)  29.5 us
    all_gather x1, waiting for transfers between devices, per_device(): lax.all_gather(key_updated.astype(jnp.bfloat16), 'fs', axis=0, tiled=True)  14 us
    unnamed x46, local copies, waits for them, and re-layouts  10.9 us
  transfers between devices with their start and end apart: 6, of which 6 were waited for; matrix products, arithmetic and copies ran while one was open for 3% of the time, Pallas kernels for 0%

profile of v1, /device:TPU:0, one launch (start us, length us, event | category | flops | bytes accessed | tf_op | source)
XLA Modules:
  0.0 323.3 jit_solution(8288501356079745393)
XLA Ops:
  7.3 2.7 convolution_bitcast_fusion
  10.0 2.2 convolution_bitcast_fusion.1
  12.2 1.3 convolution_bitcast_fusion.2
  13.5 65.0 %all-reduce.6.cloned.1.call-done = (f32[1024,128]{0,1:T(8,128)}, f32[1024,128]{0,1:T(8,128)}, f32[1024,128]{0,1:T(8,128)}) async-done(((f32[1024,128]{0,1:T(8,128)}, f32[1024,128]{0,1:T(8,128)}, f32[1024,128]{0,1:T(8,128)}), (f32[1024,128]{0,1:T(8,128)}, f32[1024,128]{0,1:T(8,128)}, f32[1024,128]{0,1:T(8,128)})) %all-reduce.6.cloned.1.call-update) | async-done | bytes 1572880 | tf_op jit(solution)/shard_map/psum | solution.py:63
  78.6 2.4 convolution_bitcast_fusion.3
  81.0 1.3 fusion.36
  82.3 1.0 fusion.37
  83.4 45.7 %all-reduce.8.cloned.1.call-done = (f32[128,512]{1,0:T(8,128)}, f32[512,128]{0,1:T(8,128)}, f32[128,128]{1,0:T(8,128)}) async-done(((f32[128,512]{1,0:T(8,128)}, f32[512,128]{0,1:T(8,128)}, f32[128,128]{1,0:T(8,128)}), (f32[128,512]{1,0:T(8,128)}, f32[512,128]{0,1:T(8,128)}, f32[128,128]{1,0:T(8,128)})) %all-reduce.8.cloned.1.call-update) | async-done | bytes 589840 | tf_op jit(solution)/shard_map/psum | solution.py:75
  129.1 1.6 multiply_reduce_fusion
  130.8 1.1 copy.35
  131.8 1.6 multiply_reduce_fusion.1
  133.5 1.5 multiply_reduce_fusion.2
  136.9 0.7 concatenate.3.clone
  137.7 29.5 %all-gather.12.cloned.1.call-done = f32[4160,128]{1,0:T(8,128)} async-done(((f32[520,128]{1,0:T(8,128)}), f32[4160,128]{1,0:T(8,128)}) %all-gather.12.cloned.1.call-update) | async-done | bytes 2129936 | tf_op jit(solution)/shard_map/all_gather | solution.py:83
  167.2 1.5 slice_reduce_fusion
  169.4 0.9 fusion.19
  170.4 2.6 fusion.34
  173.1 0.1 slice.9
  173.3 0.8 copy-done.14
  174.1 0.2 copy-done.15
  174.3 0.2 fusion
  174.5 0.6 copy-done.5
  175.1 3.5 %fusion.33 = (bf16[1024,512]{1,0:T(8,128)(2,1)}, f32[1024,512]{1,0:T(8,128)}, f32[1024,512]{1,0:T(8,128)}) fusion(f32[1024,512]{1,0:T(8,128)S(1)} %copy-done.5, bf16[4096,128]{1,0:T(8,128)(2,1)S(1)} %copy-done, s32[]{:T(128)S(6)} %select_n.5, f32[1024,128]{1,0:T(8,128)S(1)} %get-tuple-element.64, f32[1024,128]{1,0:T(8,128)S(1)} %get-tuple-element.65), kind=kOutput, calls=%fused_computation.51 | convolution fusion | flops 807141376 | bytes 8519684 | tf_op jit(solution)/shard_map/dot_general | solution.py:102
  178.7 1.4 fusion.5
  180.1 0.5 copy-done.6
  180.5 4.5 %fusion.35 = (bf16[1024,512]{1,0:T(8,128)(2,1)}, f32[1024,512]{1,0:T(8,128)}, f32[1024,512]{1,0:T(8,128)}) fusion(f32[1024,512]{1,0:T(8,128)S(1)} %copy-done.6, f32[128,512]{1,0:T(8,128)S(1)} %get-tuple-element.60, f32[128,512]{1,0:T(8,128)S(1)} %get-tuple-element.61, bf16[4096,128]{1,0:T(8,128)(2,1)} %param.25, s32[]{:T(128)S(6)} %select_n.4), kind=kOutput, calls=%fused_computation.53 | convolution fusion | flops 807010304 | bytes 8126468 | tf_op jit(solution)/shard_map/dot_general | solution.py:100
  185.1 14.0 %all-gather.8.cloned.1.call-done = bf16[4096,128]{1,0:T(8,128)(2,1)} async-done(((bf16[1024,128]{1,0:T(8,128)(2,1)}), bf16[4096,128]{1,0:T(8,128)(2,1)}) %all-gather.8.cloned.1.call-update) | async-done | bytes 1048592 | tf_op jit(solution)/shard_map/all_gather | solution.py:108
  199.1 54.9 %all-gather.10.cloned.1.call-done = bf16[4096,512]{1,0:T(8,128)(2,1)} async-done(((bf16[1024,512]{1,0:T(8,128)(2,1)}), bf16[4096,512]{1,0:T(8,128)(2,1)}) %all-gather.10.cloned.1.call-update) | async-done | bytes 4194320 | tf_op jit(solution)/shard_map/all_gather | solution.py:109
  253.9 54.9 %all-gather.6.cloned.1.call-done = bf16[4096,512]{1,0:T(8,128)(2,1)} async-done(((bf16[1024,512]{1,0:T(8,128)(2,1)}), bf16[4096,512]{1,0:T(8,128)(2,1)}) %all-gather.6.cloned.1.call-update) | async-done | bytes 4194320 | tf_op jit(solution)/shard_map/all_gather | solution.py:107
  308.8 4.6 %copy.45 = bf16[4096,512]{1,0:T(8,128)(2,1)} copy(bf16[4096,512]{1,0:T(8,128)(2,1)} %all-gather.6.cloned.1.call-done) | data formatting | bytes 8388608
  313.5 1.0 copy.46
  314.4 2.0 copy.47
  (50 shorter events, 0.5 us)
Async XLA Ops:
  7.2 5.0 %copy-start = (bf16[4096,128]{1,0:T(8,128)(2,1)S(1)}, bf16[4096,128]{1,0:T(8,128)(2,1)}, u32[]{:S(2)}) copy-start(bf16[4096,128]{1,0:T(8,128)(2,1)} %param.27) | copy-start | bytes 3145732
  7.2 2.8 copy-start.1
  7.2 5.0 %copy-start.10 = (bf16[1024,512]{1,0:T(8,128)(2,1)S(1)}, bf16[1024,512]{1,0:T(8,128)(2,1)}, u32[]{:S(2)}) copy-start(bf16[1024,512]{1,0:T(8,128)(2,1)} %param.21) | copy-start | bytes 3145732
  7.2 71.3 %all-reduce.6.cloned.1.call-start = ((), (), s32[]{:S(2)}) async-start(), calls=%async_computation.4 | async-start | bytes 3145728 | tf_op jit(solution)/shard_map/psum | solution.py:63
  12.2 66.4 %copy-start.11 = (bf16[1024,512]{1,0:T(8,128)(2,1)S(1)}, bf16[1024,512]{1,0:T(8,128)(2,1)}, u32[]{:S(2)}) copy-start(bf16[1024,512]{1,0:T(8,128)(2,1)} %param.20) | copy-start | bytes 3145732
  13.5 67.5 %copy-start.12 = (bf16[1024,512]{1,0:T(8,128)(2,1)S(1)}, bf16[1024,512]{1,0:T(8,128)(2,1)}, u32[]{:S(2)}) copy-start(bf16[1024,512]{1,0:T(8,128)(2,1)} %param.18) | copy-start | bytes 3145732
  13.5 68.8 %copy-start.20 = (bf16[1024,128]{1,0:T(8,128)(2,1)S(1)}, bf16[1024,128]{1,0:T(8,128)(2,1)}, u32[]{:S(2)}) copy-start(bf16[1024,128]{1,0:T(8,128)(2,1)} %param.19) | copy-start | bytes 786436
  13.5 115.6 %all-reduce.8.cloned.1.call-start = ((), (), s32[]{:S(2)}) async-start(), calls=%async_computation.5 | async-start | bytes 1179648 | tf_op jit(solution)/shard_map/psum | solution.py:75
  78.6 2.4 copy-start.16
  78.6 3.8 %copy-start.17 = (f32[1024,128]{0,1:T(8,128)S(1)}, f32[1024,128]{0,1:T(8,128)}, u32[]{:S(2)}) copy-start(f32[1024,128]{0,1:T(8,128)} %get-tuple-element.17) | copy-start | bytes 1572868
  83.3 83.8 %all-gather.12.cloned.1.call-start = ((), (), s32[]{:S(2)}) async-start(), calls=%async_computation.3 | async-start | bytes 2396160 | tf_op jit(solution)/shard_map/all_gather | solution.py:83
  137.6 61.5 %all-gather.8.cloned.1.call-start = ((), (), s32[]{:S(2)}) async-start(), calls=%async_computation.1 | async-start | bytes 1310720 | tf_op jit(solution)/shard_map/all_gather | solution.py:108
  167.2 5.9 %copy-start.7 = (f32[4160,128]{1,0:T(8,128)S(1)}, f32[4160,128]{1,0:T(8,128)}, u32[]{:S(2)}) copy-start(f32[4160,128]{1,0:T(8,128)} %all-gather.12.cloned.1.call-done) | copy-start | bytes 6389764
  170.4 2.9 copy-start.18
  170.4 2.9 copy-start.19
  173.0 80.9 %all-gather.10.cloned.1.call-start = ((), (), s32[]{:S(2)}) async-start(), calls=%async_computation.2 | async-start | bytes 5242880 | tf_op jit(solution)/shard_map/all_gather | solution.py:109
  173.1 1.0 copy-start.14
  173.1 1.2 copy-start.15
  173.3 1.8 copy-start.5
  174.5 4.1 %copy-start.3 = (f32[1024,128]{1,0:T(8,128)}, f32[1024,128]{1,0:T(8,128)S(1)}, u32[]{:S(2)}) copy-start(f32[1024,128]{1,0:T(8,128)S(1)} %get-tuple-element.65) | copy-start | bytes 1572868
  174.5 4.1 %copy-start.4 = (f32[1024,128]{1,0:T(8,128)}, f32[1024,128]{1,0:T(8,128)S(1)}, u32[]{:S(2)}) copy-start(f32[1024,128]{1,0:T(8,128)S(1)} %get-tuple-element.64) | copy-start | bytes 1572868
  178.6 1.9 copy-start.6
  178.6 130.2 %all-gather.6.cloned.1.call-start = ((), (), s32[]{:S(2)}) async-start(), calls=%async_computation | async-start | bytes 5242880 | tf_op jit(solution)/shard_map/all_gather | solution.py:107
  180.0 5.0 %copy-start.8 = (f32[128,512]{1,0:T(8,128)}, f32[128,512]{1,0:T(8,128)S(1)}, u32[]{:S(2)}) copy-start(f32[128,512]{1,0:T(8,128)S(1)} %get-tuple-element.61) | copy-start | bytes 786436
  180.1 5.0 %copy-start.9 = (f32[128,512]{1,0:T(8,128)}, f32[128,512]{1,0:T(8,128)S(1)}, u32[]{:S(2)}) copy-start(f32[128,512]{1,0:T(8,128)S(1)} %get-tuple-element.60) | copy-start | bytes 786436
  308.8 4.6 %copy-start.13 = (bf16[4096,128]{1,0:T(8,128)(2,1)S(1)}, bf16[4096,128]{1,0:T(8,128)(2,1)}, u32[]{:S(2)}) copy-start(bf16[4096,128]{1,0:T(8,128)(2,1)} %all-gather.8.cloned.1.call-done) | copy-start | bytes 3145732
  308.8 5.6 %copy-start.2 = (bf16[4096,512]{1,0:T(8,128)(2,1)S(1)}, bf16[4096,512]{1,0:T(8,128)(2,1)}, u32[]{:S(2)}) copy-start(bf16[4096,512]{1,0:T(8,128)(2,1)} %all-gather.10.cloned.1.call-done) | copy-start | bytes 12582916
Sparse Core Ops, SparseCore 0:
  13.6 64.9 all-reduce.5
  83.5 45.6 all-reduce.7
  137.7 29.4 all-gather.11
  173.2 25.8 all-gather.7
  201.3 52.5 all-gather.9
  256.2 52.5 all-gather.5

commit v2 on v1

--- a/solution.py
+++ b/solution.py
@@ -1,6 +1,10 @@
+import functools
+
 import jax
 import jax.numpy as jnp
 from jax import lax
+from jax.experimental import pallas as pl
+from jax.experimental.pallas import tpu as pltpu
 from jax.sharding import PartitionSpec as P
 
 LEARN = 0.02
@@ -25,6 +29,284 @@
         precision=precision,
         preferred_element_type=jnp.float32,
     )
+
+
+def split_three(values):
+    high = values.astype(jnp.bfloat16)
+    rest = values - high.astype(jnp.float32)
+    middle = rest.astype(jnp.bfloat16)
+    low = (rest - middle.astype(jnp.float32)).astype(jnp.bfloat16)
+    return high, middle, low
+
+
+class Sender:
+    def __init__(self, send_sem, recv_sem):
+        self.send_sem, self.recv_sem, self.used, self.started = send_sem, recv_sem, 0, []
+
+    def start(self, source, target, device):
+        copy = pltpu.make_async_remote_copy(
+            src_ref=source,
+            dst_ref=target,
+            send_sem=self.send_sem.at[self.used],
+            recv_sem=self.recv_sem.at[self.used],
+            device_id=device,
+            device_id_type=pl.DeviceIdType.MESH,
+        )
+        self.used += 1
+        copy.start()
+        self.started.append(copy)
+        return copy
+
+    def drain(self):
+        for copy in self.started:
+            copy.wait_send()
+
+
+def greet(nf, nt, row, col, both):
+    barrier = pltpu.get_barrier_semaphore()
+    peers = [{"fs": lax.rem(row + o, nf), "tp": col} for o in range(1, nf)]
+    if both:
+        peers += [{"fs": row, "tp": lax.rem(col + o, nt)} for o in range(1, nt)]
+    for peer in peers:
+        pl.semaphore_signal(
+            barrier, inc=1, device_id=peer, device_id_type=pl.DeviceIdType.MESH
+        )
+    pl.semaphore_wait(barrier, len(peers))
+
+
+def reduce_kernel(
+    nf, nt,
+    x_ref, qu_ref, ku_ref, h_ref, bu_ref, qb_ref, kb_ref, bb_ref,
+    qk_out, b_out, total_out,
+    part, from_pair, halves, arrived, whole, other,
+    part_qk, part_b, got_qk, got_b, all_qk, all_b, spread_b, sums,
+    send_sem, recv_sem,
+):
+    row, col = lax.axis_index("fs"), lax.axis_index("tp")
+    core, height = lax.rem(col, 2), lax.div(col, 2)
+    nz = nt // 2
+    rank = qb_ref.shape[1]
+    half = x_ref.shape[0] // 2
+    piece = half // nz
+    query_cols = qu_ref.shape[1]
+    greet(nf, nt, row, col, True)
+    sender = Sender(send_sem, recv_sem)
+    pair = {"fs": row, "tp": height * 2 + (1 - core)}
+
+    def above(o):
+        return {"fs": row, "tp": lax.rem(height + o, nz) * 2 + core}
+
+    def beside(o):
+        return {"fs": lax.rem(row + o, nf), "tp": col}
+
+    def project(which):
+        rows = pl.ds(pl.multiple_of(which * half, half), half)
+        x = x_ref[rows, :]
+        return (
+            jnp.dot(x, qb_ref[...], preferred_element_type=jnp.float32),
+            jnp.dot(x, kb_ref[...], preferred_element_type=jnp.float32),
+            jnp.dot(bu_ref[rows, :], bb_ref[...], preferred_element_type=jnp.float32),
+        )
+
+    for n, value in enumerate(project(1 - core)):
+        part[:, n * rank : (n + 1) * rank] = value
+    swap = sender.start(part, from_pair, pair)
+    own = project(core)
+    swap.wait_recv()
+    for n, value in enumerate(own):
+        span = slice(n * rank, (n + 1) * rank)
+        halves[:, :, span] = (value + from_pair[:, span]).reshape(nz, piece, rank)
+    copies = [
+        sender.start(halves.at[lax.rem(height + o, nz)], arrived.at[o - 1], above(o))
+        for o in range(1, nz)
+    ]
+    total = halves[height]
+    for o, copy in enumerate(copies):
+        copy.wait_recv()
+        total = total + arrived[o]
+    whole[height] = total
+    copies = [sender.start(whole.at[height], whole.at[height], above(o)) for o in range(1, nz)]
+    across = [sender.start(whole.at[height], other.at[height], pair)]
+    for o, copy in enumerate(copies, 1):
+        copy.wait_recv()
+        source = lax.rem(height + nz - o, nz)
+        across.append(sender.start(whole.at[source], other.at[source], pair))
+
+    over_rows = (((0,), (0,)), ((), ()))
+
+    def low_parts(values, which):
+        rows = pl.ds(pl.multiple_of(which * half, half), half)
+        sides = (qu_ref[rows, :], ku_ref[rows, :], h_ref[rows, :])
+        parts = []
+        for n, side in enumerate(sides):
+            terms = split_three(values[:, n * rank : (n + 1) * rank])
+            parts.append(
+                sum(
+                    lax.dot_general(term, side, over_rows, preferred_element_type=jnp.float32)
+                    for term in terms
+                )
+            )
+        return parts
+
+    first = low_parts(whole[...].reshape(half, 3 * rank), core)
+    for copy in across:
+        copy.wait_recv()
+    second = low_parts(other[...].reshape(half, 3 * rank), 1 - core)
+    query_part, key_part, branch_part = [a + b for a, b in zip(first, second)]
+    part_qk[:, :, :query_cols] = query_part.reshape(nf, rank // nf, query_cols)
+    part_qk[:, :, query_cols:] = key_part.reshape(nf, rank // nf, key_part.shape[1])
+    part_b[...] = branch_part.T.reshape(part_b.shape)
+
+    copies = []
+    for o in range(1, nf):
+        to = lax.rem(row + o, nf)
+        copies.append(sender.start(part_qk.at[to], got_qk.at[o - 1], beside(o)))
+        copies.append(sender.start(part_b.at[to], got_b.at[o - 1], beside(o)))
+    for copy in copies:
+        copy.wait_recv()
+    sum_qk, sum_b = part_qk[row], part_b[row]
+    for o in range(nf - 1):
+        sum_qk = sum_qk + got_qk[o]
+        sum_b = sum_b + got_b[o]
+    rows_b = sum_b.shape[0]
+    squares = jnp.sum(sum_qk * sum_qk) + jnp.sum(sum_b * sum_b)
+    all_qk[row] = sum_qk
+    all_b[col, :rows_b, :] = sum_b
+    all_b[col, rows_b:, :] = jnp.full((8, rank), squares, jnp.float32)
+
+    copies_b = [
+        sender.start(all_b.at[col], all_b.at[col], {"fs": row, "tp": lax.rem(col + o, nt)})
+        for o in range(1, nt)
+    ]
+    copies_qk = [sender.start(all_qk.at[row], all_qk.at[row], beside(o)) for o in range(1, nf)]
+    for copy in copies_b:
+        copy.wait_recv()
+    sums[row] = jnp.sum(all_b[:, rows_b:, :], axis=0)
+    each = nt // nf
+    copies = []
+    for o in range(1, nf):
+        blocks = pl.ds(lax.rem(row + o, nf) * each, each)
+        copies.append(sender.start(sums.at[row], sums.at[row], beside(o)))
+        copies.append(sender.start(all_b.at[blocks], spread_b.at[row], beside(o)))
+    b_out[:, row] = all_b[pl.ds(row * each, each)][:, :rows_b, :]
+    for copy in copies_qk:
+        copy.wait_recv()
+    qk_out[...] = all_qk[...].reshape(qk_out.shape)
+    for copy in copies:
+        copy.wait_recv()
+    for o in range(1, nf):
+        source = lax.rem(row + o, nf)
+        b_out[:, source] = spread_b[source][:, :rows_b, :]
+    total_out[...] = jnp.sum(sums[...], axis=0)
+    sender.drain()
+
+
+def reduced(nf, nt, x, qu, ku, h, bu, qb, kb, bb):
+    tokens, features = x.shape
+    rank = qb.shape[1]
+    cols = qu.shape[1] + ku.shape[1]
+    half, nz, each = tokens // 2, nt // 2, nt // nf
+    piece, thin, rows_b = half // nz, rank // nf, features // nf
+    copies = 1 + 2 * (nz - 1) + nz + 2 * (nf - 1) + (nt - 1) + 3 * (nf - 1)
+    vmem = pl.BlockSpec(memory_space=pltpu.VMEM)
+    f32 = jnp.float32
+    return pl.pallas_call(
+        functools.partial(reduce_kernel, nf, nt),
+        out_shape=(
+            jax.ShapeDtypeStruct((rank, cols), f32),
+            jax.ShapeDtypeStruct((each, nf, rows_b, rank), f32),
+            jax.ShapeDtypeStruct((8, rank), f32),
+        ),
+        in_specs=[vmem] * 8,
+        out_specs=(vmem,) * 3,
+        scratch_shapes=[
+            pltpu.VMEM((half, 3 * rank), f32),
+            pltpu.VMEM((half, 3 * rank), f32),
+            pltpu.VMEM((nz, piece, 3 * rank), f32),
+            pltpu.VMEM((nz - 1, piece, 3 * rank), f32),
+            pltpu.VMEM((nz, piece, 3 * rank), f32),
+            pltpu.VMEM((nz, piece, 3 * rank), f32),
+            pltpu.VMEM((nf, thin, cols), f32),
+            pltpu.VMEM((nf, rows_b, rank), f32),
+            pltpu.VMEM((nf - 1, thin, cols), f32),
+            pltpu.VMEM((nf - 1, rows_b, rank), f32),
+            pltpu.VMEM((nf, thin, cols), f32),
+            pltpu.VMEM((nt, rows_b + 8, rank), f32),
+            pltpu.VMEM((nf, each, rows_b + 8, rank), f32),
+            pltpu.VMEM((nf, 8, rank), f32),
+            pltpu.SemaphoreType.DMA((copies,)),
+            pltpu.SemaphoreType.DMA((copies,)),
+        ],
+        compiler_params=pltpu.CompilerParams(
+            collective_id=0, has_side_effects=True, vmem_limit_bytes=48 * 2**20
+        ),
+    )(x, qu, ku, h, bu, qb, kb, bb)
+
+
+def gather_kernel(nf, nt, q_ref, b_ref, k_ref, q_out, b_out, k_out, send_sem, recv_sem, own_sem):
+    row, col = lax.axis_index("fs"), lax.axis_index("tp")
+    greet(nf, nt, row, col, False)
+    sender = Sender(send_sem, recv_sem)
+    pairs = ((q_ref, q_out), (b_ref, b_out), (k_ref, k_out))
+    local = []
+    if nf == 4:
+        side = row + 1 - 2 * lax.rem(row, 2)
+        front = lax.rem(row + 2, 4)
+        half = q_ref.shape[0] // 2
+        names = ({"fs": side, "tp": col}, {"fs": front, "tp": col})
+        forwards = []
+        for ref, out in pairs:
+            for h in range(2):
+                rows = pl.ds(h * half, half)
+                for n in ((0, 1), (1, 0))[h]:
+                    copy = sender.start(ref.at[rows], out.at[row, rows], names[n])
+                    forwards.append((n, h, out, copy))
+        for n, (ref, out) in enumerate(pairs):
+            local.append(pltpu.make_async_copy(ref, out.at[row], own_sem.at[n]))
+            local[-1].start()
+        last = []
+        for n, h, out, copy in forwards:
+            copy.wait_recv()
+            if n == h:
+                source = (side, front)[n]
+                held = out.at[source, pl.ds(h * half, half)]
+                last.append(sender.start(held, held, names[1 - n]))
+        for copy in last:
+            copy.wait_recv()
+    else:
+        copies = [
+            sender.start(ref, out.at[row], {"fs": lax.rem(row + o, nf), "tp": col})
+            for ref, out in pairs
+            for o in range(1, nf)
+        ]
+        for n, (ref, out) in enumerate(pairs):
+            local.append(pltpu.make_async_copy(ref, out.at[row], own_sem.at[n]))
+            local[-1].start()
+        for copy in copies:
+            copy.wait_recv()
+    for copy in local:
+        copy.wait()
+    sender.drain()
+
+
+def gathered_rows(nf, nt, *blocks):
+    count = 18 if nf == 4 else 3 * (nf - 1)
+    wide = [jax.ShapeDtypeStruct((nf, *block.shape), block.dtype) for block in blocks]
+    outs = pl.pallas_call(
+        functools.partial(gather_kernel, nf, nt),
+        out_shape=tuple(wide),
+        in_specs=[pl.BlockSpec(memory_space=pltpu.VMEM)] * 3,
+        out_specs=(pl.BlockSpec(memory_space=pl.ANY),) * 3,
+        scratch_shapes=[
+            pltpu.SemaphoreType.DMA((count,)),
+            pltpu.SemaphoreType.DMA((count,)),
+            pltpu.SemaphoreType.DMA((3,)),
+        ],
+        compiler_params=pltpu.CompilerParams(
+            collective_id=1, has_side_effects=True, vmem_limit_bytes=16 * 2**20
+        ),
+    )(*blocks)
+    return [out.reshape(-1, out.shape[-1]) for out in outs]
 
 
 def per_device(
@@ -60,31 +342,24 @@
         return lax.dynamic_slice_in_dim(basis, col_index * features, features, 0)
 
     block_branch = own_block(branch_basis)
-    proj_query, proj_key, proj_branch = lax.psum(
-        (
-            jnp.dot(normed_inputs, own_block(query_basis), preferred_element_type=jnp.float32),
-            jnp.dot(normed_inputs, own_block(key_basis), preferred_element_type=jnp.float32),
-            jnp.dot(branch_upstream, block_branch, preferred_element_type=jnp.float32),
-        ),
-        "tp",
-    )
-    part_query = over_tokens(proj_query, query_upstream.astype(jnp.float32), exact)
-    part_key = over_tokens(proj_key, key_upstream.astype(jnp.float32), exact)
-    part_branch = over_tokens(head_outputs.astype(jnp.float32), proj_branch, exact)
     own_branch = block_branch.astype(jnp.float32)
-    query_low, key_low, branch_block = lax.psum((part_query, part_key, part_branch), "fs")
-    local_squares = (
-        jnp.sum(query_low * query_low)
-        + jnp.sum(key_low * key_low)
-        + jnp.sum(branch_block * branch_block)
-    )
-    rows_block = branch_block.shape[0]
-    carried = jnp.concatenate([branch_block, jnp.full((8, rank), local_squares)], axis=0)
-    gathered = lax.all_gather(carried, "tp", axis=0)
-    total = jnp.sum(gathered[:, rows_block, 0])
-    branch_all = gathered[:, :rows_block, :].reshape(n_cols * rows_block, rank)
-    own_rows = branch_first.shape[0]
-    branch_low = lax.dynamic_slice_in_dim(branch_all, row_index * own_rows, own_rows, 0)
+    lanes = -key_local % 128
+    low, branch_low, squares = reduced(
+        n_rows,
+        n_cols,
+        normed_inputs,
+        query_upstream,
+        jnp.pad(key_upstream, ((0, 0), (0, lanes))),
+        head_outputs,
+        branch_upstream,
+        own_block(query_basis),
+        own_block(key_basis),
+        block_branch,
+    )
+    query_low = low[:, :query_local]
+    key_low = low[:, query_local : query_local + key_local]
+    branch_low = branch_low.reshape(branch_first.shape)
+    total = squares[0, 0]
     entries = rank * n_cols * (2 * query_local + key_local)
     rms_value = jnp.sqrt(total / float(entries))
     clip = 1.0 / jnp.maximum(1.0, rms_value / CLIP_RMS)
@@ -103,11 +378,14 @@
     query_updated = query_master - LEARN * query_step
     key_updated = key_master - LEARN * key_step
     branch_updated = branch_master - LEARN * branch_step
-    query_copy, key_copy, branch_copy = (
-        lax.all_gather(query_updated.astype(jnp.bfloat16), "fs", axis=0, tiled=True),
-        lax.all_gather(key_updated.astype(jnp.bfloat16), "fs", axis=0, tiled=True),
-        lax.all_gather(branch_updated.astype(jnp.bfloat16), "fs", axis=0, tiled=True),
-    )
+    query_copy, branch_copy, key_copy = gathered_rows(
+        n_rows,
+        n_cols,
+        query_updated.astype(jnp.bfloat16),
+        branch_updated.astype(jnp.bfloat16),
+        jnp.pad(key_updated, ((0, 0), (0, lanes))).astype(jnp.bfloat16),
+    )
+    key_copy = key_copy[:, :key_local]
     return (
         query_step,
         key_step,

time: 324 us -> 180 us (0.56)
  waiting for transfers between devices: 264 us -> 0 us
  Pallas kernels: 0 us -> 152 us
  between operations: 17 us -> 1.62 us
  matrix products: 21.6 us -> 9 us
  other arithmetic: 8.68 us -> 0.3 us
    all_gather x4 -> x0, waiting for transfers between devices: 153 us -> none  [the longest x1 54.9 us: per_device(): lax.all_gather(query_updated.astype(jnp.bfloat16), 'fs', axis=0, tiled=True)]
    pallas_call x0 -> x2, Pallas kernels: none -> 152 us  [the longest x1 81 us: gathered_rows(): pl.pallas_call(functools.partial(gather_kernel, nf, nt), out_shape=tuple(...]
    psum x2 -> x0, waiting for transfers between devices: 111 us -> none  [the longest x1 65 us: per_device(): lax.psum((jnp.dot(normed_inputs, own_block(query_basis), preferred_elemen...]
    dot_general x6 -> x0, matrix products: 10.9 us -> none  [the longest x3 4.75 us: over_tokens(): lax.dot_general(left, right, (((0,), (0,)), ((), ())), precision=precisio...]
    reduce_sum x4 -> x0, other arithmetic: 6.23 us -> none  [the longest x1 1.63 us: per_device(): jnp.sum(query_low * query_low) + jnp.sum(key_low * key_low)]
    unnamed x46 -> x45, local copies, waits for them, and re-layouts: 10.9 us -> 12.8 us
  transfers between devices with their start and end apart: 6 -> 0, of which waited for: 6 -> 0; matrix products, arithmetic and copies ran while one was open for 3% -> 0% of each run, Pallas kernels for 0% -> 0%
where the time goes in v2:
time: 180 us; the launch traced here: 177 us
  Pallas kernels  152 us (84%)
  local copies, waits for them, and re-layouts  14.3 us (8%)
  matrix products  9 us (5%)
    pallas_call x1, Pallas kernels, gathered_rows(): pl.pallas_call(functools.partial(gather_kernel, nf, nt), out_shape=tuple(...  81 us
    pallas_call x1, Pallas kernels, reduced(): pl.pallas_call(functools.partial(reduce_kernel, nf, nt), out_shape=(jax.S...  70.8 us
    unnamed x45, local copies, waits for them, and re-layouts  12.8 us

profile of v2, /device:TPU:0, one launch (start us, length us, event | category | flops | bytes accessed | tf_op | source)
XLA Modules:
  0.0 177.0 jit_solution(8920082290635509439)
XLA Ops:
  0.6 0.0 copy-start
  0.7 1.2 copy-done
  1.9 1.0 constant_dynamic-slice_fusion
  2.9 0.0 copy-start.1
  2.9 1.2 copy-done.1
  4.1 1.2 copy-done.2
  5.3 1.2 copy-done.3
  6.6 1.2 copy-done.4
  7.8 0.9 copy-done.5
  8.8 70.8 %shard_map.280 = (f32[128,640]{1,0:T(8,128)S(1)}, f32[2,4,128,128]{3,2,1,0:T(8,128)S(1)}, f32[8,128]{1,0:T(8,128)S(1)}) custom-call(bf16[1024,512]{1,0:T(8,128)(2,1)S(1)} %copy-done.1, bf16[1024,512]{1,0:T(8,128)(2,1)S(1)} %copy-done.2, bf16[1024,128]{1,0:T(8,128)(2,1)S(1)} %copy-done.5, bf16[1024,512]{1,0:T(8,128)(2,1)S(1)} %copy-done.3, ...), custom_call_target="tpu_custom_call" | custom-call | tf_op jit(solution)/shard_map/pallas_call | solution.py:213
  79.5 0.0 copy-start.12
  79.5 0.0 copy-start.13
  79.5 0.5 slice.9
  80.9 0.0 copy-start.14
  80.9 0.0 copy-start.17
  80.9 0.0 copy-start.18
  81.0 0.1 fusion.6
  81.0 0.0 copy-start.10
  81.1 0.0 copy-start.11
  81.1 0.0 copy-start.8
  81.1 0.2 fusion
  81.3 0.0 copy-start.6
  81.3 0.0 copy-start.7
  81.3 0.7 copy-done.14
  82.0 2.6 %fusion.26 = (bf16[1024,128]{1,0:T(8,128)(2,1)S(1)}, f32[1024,128]{1,0:T(8,128)}, f32[1024,128]{1,0:T(8,128)}) fusion(f32[1024,128]{1,0:T(8,128)S(1)} %copy-done.14, f32[128,128]{1,0:T(8,128)S(1)} %get-tuple-element.70, f32[128,128]{1,0:T(8,128)S(1)} %get-tuple-element.71, bf16[4096,128]{1,0:T(8,128)(2,1)} %param.26, s32[]{:T(128)S(6)} %select_n.4), kind=kOutput, calls=%fused_computation.41 | convolution fusion | flops 201752576 | bytes 2228228 | tf_op jit(solution)/shard_map/dot_general | solution.py:376
  84.6 0.0 copy-start.9
  84.6 3.1 %fusion.27 = (bf16[1024,512]{1,0:T(8,128)(2,1)S(1)}, f32[1024,512]{1,0:T(8,128)}, f32[1024,512]{1,0:T(8,128)}) fusion(f32[1024,512]{1,0:T(8,128)S(1)} %copy-done.8, bf16[512,128]{1,0:T(8,128)(2,1)S(1)} %get-tuple-element.42.bb_ref, f32[1024,128]{1,0:T(8,128)S(1)} %get-tuple-element.72, f32[1024,128]{1,0:T(8,128)S(1)} %get-tuple-element.73), kind=kOutput, calls=%fused_computation.42 | convolution fusion | flops 807141376 | bytes 8519680 | tf_op jit(solution)/shard_map/dot_general | solution.py:377
  87.8 3.2 %fusion.28 = (bf16[1024,512]{1,0:T(8,128)(2,1)S(1)}, f32[1024,512]{1,0:T(8,128)}, f32[1024,512]{1,0:T(8,128)}) fusion(f32[1024,512]{1,0:T(8,128)S(1)} %copy-done.9, f32[128,512]{1,0:T(8,128)S(1)} %get-tuple-element.68, f32[128,512]{1,0:T(8,128)S(1)} %get-tuple-element.69, bf16[4096,128]{1,0:T(8,128)(2,1)S(1)} %copy-done, s32[]{:T(128)S(6)} %select_n.4), kind=kOutput, calls=%fused_computation.43 | convolution fusion | flops 807010304 | bytes 8126468 | tf_op jit(solution)/shard_map/dot_general | solution.py:375
  91.0 81.0 %shard_map.281 = (bf16[4,1024,512]{2,1,0:T(8,128)(2,1)S(1)}, bf16[4,1024,512]{2,1,0:T(8,128)(2,1)S(1)}, bf16[4,1024,128]{2,1,0:T(8,128)(2,1)S(1)}) custom-call(bf16[1024,512]{1,0:T(8,128)(2,1)S(1)} %get-tuple-element.31.q_ref, bf16[1024,512]{1,0:T(8,128)(2,1)S(1)} %get-tuple-element.29.b_ref, bf16[1024,128]{1,0:T(8,128)(2,1)S(1)} %get-tuple-element.27.k_ref), custom_call_target="tpu_custom_call" | custom-call | tf_op jit(solution)/shard_map/pallas_call | solution.py:295
  172.0 2.0 %copy.35 = bf16[4096,512]{1,0:T(8,128)(2,1)} copy(bf16[4096,512]{1,0:T(8,128)(2,1)S(1)} %bitcast.11) | data formatting | bytes 8388608
  174.0 1.0 copy.36
  175.0 2.0 %copy.37 = bf16[4096,512]{1,0:T(8,128)(2,1)} copy(bf16[4096,512]{1,0:T(8,128)(2,1)S(1)} %bitcast.10) | data formatting | bytes 8388608
  (25 shorter events, 0.1 us)
Async XLA Ops:
  0.6 1.2 copy-start
  2.9 1.2 copy-start.1
  4.1 1.2 copy-start.2
  5.3 1.2 copy-start.3
  6.6 1.2 copy-start.4
  7.8 0.9 copy-start.5
  8.7 72.1 %copy-start.19 = (f32[128,128]{1,0:T(8,128)S(1)}, f32[128,128]{1,0:T(8,128)}, u32[]{:S(2)}) copy-start(f32[128,128]{1,0:T(8,128)} %param.31) | copy-start | bytes 196612
  8.7 72.1 %copy-start.20 = (f32[128,128]{1,0:T(8,128)S(1)}, f32[128,128]{1,0:T(8,128)}, u32[]{:S(2)}) copy-start(f32[128,128]{1,0:T(8,128)} %param.30) | copy-start | bytes 196612
  8.7 72.2 %copy-start.15 = (f32[128,512]{1,0:T(8,128)S(1)}, f32[128,512]{1,0:T(8,128)}, u32[]{:S(2)}) copy-start(f32[128,512]{1,0:T(8,128)} %param.29) | copy-start | bytes 786436
  8.7 72.2 %copy-start.16 = (f32[128,512]{1,0:T(8,128)S(1)}, f32[128,512]{1,0:T(8,128)}, u32[]{:S(2)}) copy-start(f32[128,512]{1,0:T(8,128)} %param.28) | copy-start | bytes 786436
  79.5 1.5 copy-start.12
  79.5 1.5 copy-start.13
  80.9 1.1 copy-start.14
  80.9 3.7 %copy-start.17 = (f32[128,128]{1,0:T(8,128)}, f32[128,128]{1,0:T(8,128)S(1)}, u32[]{:S(2)}) copy-start(f32[128,128]{1,0:T(8,128)S(1)} %get-tuple-element.71) | copy-start | bytes 196612
  80.9 3.7 %copy-start.18 = (f32[128,128]{1,0:T(8,128)}, f32[128,128]{1,0:T(8,128)S(1)}, u32[]{:S(2)}) copy-start(f32[128,128]{1,0:T(8,128)S(1)} %get-tuple-element.70) | copy-start | bytes 196612
  81.0 6.7 %copy-start.10 = (f32[128,512]{1,0:T(8,128)}, f32[128,512]{1,0:T(8,128)S(1)}, u32[]{:S(2)}) copy-start(f32[128,512]{1,0:T(8,128)S(1)} %get-tuple-element.69) | copy-start | bytes 786436
  81.1 6.7 %copy-start.11 = (f32[128,512]{1,0:T(8,128)}, f32[128,512]{1,0:T(8,128)S(1)}, u32[]{:S(2)}) copy-start(f32[128,512]{1,0:T(8,128)S(1)} %get-tuple-element.68) | copy-start | bytes 786436
  81.1 3.5 %copy-start.8 = (f32[1024,512]{1,0:T(8,128)S(1)}, f32[1024,512]{1,0:T(8,128)}, u32[]{:S(2)}) copy-start(f32[1024,512]{1,0:T(8,128)} %param.24) | copy-start | bytes 6291460
  81.3 6.5 %copy-start.6 = (f32[1024,128]{1,0:T(8,128)}, f32[1024,128]{1,0:T(8,128)S(1)}, u32[]{:S(2)}) copy-start(f32[1024,128]{1,0:T(8,128)S(1)} %get-tuple-element.73) | copy-start | bytes 1572868
  81.3 6.5 %copy-start.7 = (f32[1024,128]{1,0:T(8,128)}, f32[1024,128]{1,0:T(8,128)S(1)}, u32[]{:S(2)}) copy-start(f32[1024,128]{1,0:T(8,128)S(1)} %get-tuple-element.72) | copy-start | bytes 1572868
  84.6 3.2 %copy-start.9 = (f32[1024,512]{1,0:T(8,128)S(1)}, f32[1024,512]{1,0:T(8,128)}, u32[]{:S(2)}) copy-start(f32[1024,512]{1,0:T(8,128)} %param.22) | copy-start | bytes 6291460

commit v3 on v2

--- a/solution.py
+++ b/solution.py
@@ -74,13 +74,20 @@
     pl.semaphore_wait(barrier, len(peers))
 
 
+def square(row, col):
+    side = row + 1 - 2 * lax.rem(row, 2)
+    front = lax.rem(row + 2, 4)
+    return side, front, ({"fs": side, "tp": col}, {"fs": front, "tp": col})
+
+
 def reduce_kernel(
     nf, nt,
-    x_ref, qu_ref, ku_ref, h_ref, bu_ref, qb_ref, kb_ref, bb_ref,
-    qk_out, b_out, total_out,
+    x_hbm, qu_hbm, ku_hbm, h_hbm, bu_hbm, master_ref, qb_ref, kb_ref, bb_ref,
+    qk_out, b_out, total_out, far_out,
+    x_ref, qu_ref, ku_ref, h_ref, bu_ref,
     part, from_pair, halves, arrived, whole, other,
     part_qk, part_b, got_qk, got_b, all_qk, all_b, spread_b, sums,
-    send_sem, recv_sem,
+    send_sem, recv_sem, load_sem,
 ):
     row, col = lax.axis_index("fs"), lax.axis_index("tp")
     core, height = lax.rem(col, 2), lax.div(col, 2)
@@ -89,6 +96,20 @@
     half = x_ref.shape[0] // 2
     piece = half // nz
     query_cols = qu_ref.shape[1]
+    loads = []
+
+    def load(source, target):
+        copy = pltpu.make_async_copy(source, target, load_sem.at[len(loads)])
+        copy.start()
+        loads.append(copy)
+
+    for which in (1 - core, core):
+        rows = pl.ds(pl.multiple_of(which * half, half), half)
+        load(x_hbm.at[rows], x_ref.at[rows])
+        load(bu_hbm.at[rows], bu_ref.at[rows])
+    load(qu_hbm, qu_ref)
+    load(ku_hbm, ku_ref)
+    load(h_hbm, h_ref)
     greet(nf, nt, row, col, True)
     sender = Sender(send_sem, recv_sem)
     pair = {"fs": row, "tp": height * 2 + (1 - core)}
@@ -108,9 +129,27 @@
             jnp.dot(bu_ref[rows, :], bb_ref[...], preferred_element_type=jnp.float32),
         )
 
+    early = far_out.shape[1]
+    sent = []
+    if nf == 4:
+        side, front, names = square(row, col)
+        for turn in range(2):
+            for n in range(2):
+                rows = pl.ds((turn ^ n) * (early // 2), early // 2)
+                sent.append(
+                    sender.start(master_ref.at[rows], far_out.at[row, rows], names[n])
+                )
+    else:
+        rows = pl.ds(0, early)
+        for o in range(1, nf):
+            sent.append(sender.start(master_ref.at[rows], far_out.at[row], beside(o)))
+    loads[0].wait()
+    loads[1].wait()
     for n, value in enumerate(project(1 - core)):
         part[:, n * rank : (n + 1) * rank] = value
     swap = sender.start(part, from_pair, pair)
+    loads[2].wait()
+    loads[3].wait()
     own = project(core)
     swap.wait_recv()
     for n, value in enumerate(own):
@@ -127,6 +166,12 @@
     whole[height] = total
     copies = [sender.start(whole.at[height], whole.at[height], above(o)) for o in range(1, nz)]
     across = [sender.start(whole.at[height], other.at[height], pair)]
+    passed = []
+    if nf == 4:
+        for n, source in ((0, side), (1, front)):
+            sent[n].wait_recv()
+            held = far_out.at[source, pl.ds(n * (early // 2), early // 2)]
+            passed.append(sender.start(held, held, names[1 - n]))
     for o, copy in enumerate(copies, 1):
         copy.wait_recv()
         source = lax.rem(height + nz - o, nz)
@@ -148,6 +193,8 @@
             )
         return parts
 
+    for copy in loads[4:]:
+        copy.wait()
     first = low_parts(whole[...].reshape(half, 3 * rank), core)
     for copy in across:
         copy.wait_recv()
@@ -198,16 +245,20 @@
         source = lax.rem(row + o, nf)
         b_out[:, source] = spread_b[source][:, :rows_b, :]
     total_out[...] = jnp.sum(sums[...], axis=0)
+    for copy in (sent[2:] + passed) if nf == 4 else sent:
+        copy.wait_recv()
     sender.drain()
 
 
-def reduced(nf, nt, x, qu, ku, h, bu, qb, kb, bb):
+def reduced(nf, nt, early, x, qu, ku, h, bu, master, qb, kb, bb):
     tokens, features = x.shape
     rank = qb.shape[1]
     cols = qu.shape[1] + ku.shape[1]
     half, nz, each = tokens // 2, nt // 2, nt // nf
     piece, thin, rows_b = half // nz, rank // nf, features // nf
     copies = 1 + 2 * (nz - 1) + nz + 2 * (nf - 1) + (nt - 1) + 3 * (nf - 1)
+    copies += 6 if nf == 4 else nf - 1
+    any_place = pl.BlockSpec(memory_space=pl.ANY)
     vmem = pl.BlockSpec(memory_space=pltpu.VMEM)
     f32 = jnp.float32
     return pl.pallas_call(
@@ -216,10 +267,12 @@
             jax.ShapeDtypeStruct((rank, cols), f32),
             jax.ShapeDtypeStruct((each, nf, rows_b, rank), f32),
             jax.ShapeDtypeStruct((8, rank), f32),
+            jax.ShapeDtypeStruct((nf, early, master.shape[1]), f32),
         ),
-        in_specs=[vmem] * 8,
-        out_specs=(vmem,) * 3,
+        in_specs=[any_place] * 6 + [vmem] * 3,
+        out_specs=(vmem, vmem, vmem, any_place),
         scratch_shapes=[
+            *[pltpu.VMEM(each_in.shape, each_in.dtype) for each_in in (x, qu, ku, h, bu)],
             pltpu.VMEM((half, 3 * rank), f32),
             pltpu.VMEM((half, 3 * rank), f32),
             pltpu.VMEM((nz, piece, 3 * rank), f32),
@@ -236,76 +289,116 @@
             pltpu.VMEM((nf, 8, rank), f32),
             pltpu.SemaphoreType.DMA((copies,)),
             pltpu.SemaphoreType.DMA((copies,)),
+            pltpu.SemaphoreType.DMA((7,)),
         ],
         compiler_params=pltpu.CompilerParams(
-            collective_id=0, has_side_effects=True, vmem_limit_bytes=48 * 2**20
+            collective_id=0, has_side_effects=True, vmem_limit_bytes=58 * 2**20
         ),
-    )(x, qu, ku, h, bu, qb, kb, bb)
-
-
-def gather_kernel(nf, nt, q_ref, b_ref, k_ref, q_out, b_out, k_out, send_sem, recv_sem, own_sem):
+    )(x, qu, ku, h, bu, master, qb, kb, bb)
+
+
+def gather_kernel(
+    nf, nt,
+    q_ref, b_ref, k_ref, far_ref, master_ref, basis_ref, dir_ref,
+    q_out, b_out, k_out,
+    held_far, held_copy, send_sem, recv_sem, own_sem, load_sem, store_sem,
+):
     row, col = lax.axis_index("fs"), lax.axis_index("tp")
+    early = far_ref.shape[1]
+    pairs = ((q_ref, q_out, early), (b_ref, b_out, 0), (k_ref, k_out, 0))
+
+    def load(o):
+        source = master_ref.at[pl.ds(0, early)] if o == 0 else far_ref.at[lax.rem(row + o, nf)]
+        copy = pltpu.make_async_copy(source, held_far.at[o % 2], load_sem.at[o])
+        copy.start()
+        return copy
+
+    coming = load(0)
     greet(nf, nt, row, col, False)
     sender = Sender(send_sem, recv_sem)
-    pairs = ((q_ref, q_out), (b_ref, b_out), (k_ref, k_out))
-    local = []
+    sent = []
     if nf == 4:
-        side = row + 1 - 2 * lax.rem(row, 2)
-        front = lax.rem(row + 2, 4)
-        half = q_ref.shape[0] // 2
-        names = ({"fs": side, "tp": col}, {"fs": front, "tp": col})
-        forwards = []
-        for ref, out in pairs:
+        side, front, names = square(row, col)
+        for ref, out, base in pairs:
+            half = ref.shape[0] // 2
             for h in range(2):
                 rows = pl.ds(h * half, half)
+                target = pl.ds(base + h * half, half)
                 for n in ((0, 1), (1, 0))[h]:
-                    copy = sender.start(ref.at[rows], out.at[row, rows], names[n])
-                    forwards.append((n, h, out, copy))
-        for n, (ref, out) in enumerate(pairs):
-            local.append(pltpu.make_async_copy(ref, out.at[row], own_sem.at[n]))
-            local[-1].start()
+                    copy = sender.start(ref.at[rows], out.at[row, target], names[n])
+                    sent.append((n, h, out, target, copy))
+    else:
+        for ref, out, base in pairs:
+            for o in range(1, nf):
+                target = out.at[row, pl.ds(base, ref.shape[0])]
+                there = {"fs": lax.rem(row + o, nf), "tp": col}
+                sent.append(sender.start(ref, target, there))
+    local = []
+    for n, (ref, out, base) in enumerate(pairs):
+        target = out.at[row, pl.ds(base, ref.shape[0])]
+        local.append(pltpu.make_async_copy(ref, target, own_sem.at[n]))
+        local[-1].start()
+
+    terms = split_three(dir_ref[...])
+    rows_all = q_out.shape[1]
+    stores = []
+    for o in range(nf):
+        source = lax.rem(row + o, nf)
+        coming.wait()
+        if o + 1 < nf:
+            coming = load(o + 1)
+        if o >= 2:
+            stores[o - 2].wait()
+        basis = basis_ref[pl.ds(pl.multiple_of(source * rows_all, rows_all), early), :]
+        step = sum(jnp.dot(basis, term, preferred_element_type=jnp.float32) for term in terms)
+        held_copy[o % 2] = (held_far[o % 2] - LEARN * step).astype(held_copy.dtype)
+        stores.append(
+            pltpu.make_async_copy(
+                held_copy.at[o % 2], q_out.at[source, pl.ds(0, early)], store_sem.at[o]
+            )
+        )
+        stores[-1].start()
+
+    if nf == 4:
         last = []
-        for n, h, out, copy in forwards:
+        for n, h, out, target, copy in sent:
             copy.wait_recv()
             if n == h:
-                source = (side, front)[n]
-                held = out.at[source, pl.ds(h * half, half)]
+                held = out.at[(side, front)[n], target]
                 last.append(sender.start(held, held, names[1 - n]))
-        for copy in last:
-            copy.wait_recv()
-    else:
-        copies = [
-            sender.start(ref, out.at[row], {"fs": lax.rem(row + o, nf), "tp": col})
-            for ref, out in pairs
-            for o in range(1, nf)
-        ]
-        for n, (ref, out) in enumerate(pairs):
-            local.append(pltpu.make_async_copy(ref, out.at[row], own_sem.at[n]))
-            local[-1].start()
-        for copy in copies:
-            copy.wait_recv()
-    for copy in local:
+        sent = last
+    for copy in sent:
+        copy.wait_recv()
+    for copy in local + stores[-2:]:
         copy.wait()
     sender.drain()
 
 
-def gathered_rows(nf, nt, *blocks):
+def gathered_rows(nf, nt, q_tail, b_block, k_block, far, master, basis, direction):
     count = 18 if nf == 4 else 3 * (nf - 1)
-    wide = [jax.ShapeDtypeStruct((nf, *block.shape), block.dtype) for block in blocks]
+    early = far.shape[1]
+    blocks = (master, b_block, k_block)
+    wide = [jax.ShapeDtypeStruct((nf, *block.shape), q_tail.dtype) for block in blocks]
+    vmem = pl.BlockSpec(memory_space=pltpu.VMEM)
+    any_place = pl.BlockSpec(memory_space=pl.ANY)
     outs = pl.pallas_call(
         functools.partial(gather_kernel, nf, nt),
         out_shape=tuple(wide),
-        in_specs=[pl.BlockSpec(memory_space=pltpu.VMEM)] * 3,
-        out_specs=(pl.BlockSpec(memory_space=pl.ANY),) * 3,
+        in_specs=[vmem] * 3 + [any_place] * 2 + [vmem] * 2,
+        out_specs=(any_place,) * 3,
         scratch_shapes=[
+            pltpu.VMEM((2, early, far.shape[2]), far.dtype),
+            pltpu.VMEM((2, early, far.shape[2]), q_tail.dtype),
             pltpu.SemaphoreType.DMA((count,)),
             pltpu.SemaphoreType.DMA((count,)),
             pltpu.SemaphoreType.DMA((3,)),
+            pltpu.SemaphoreType.DMA((nf,)),
+            pltpu.SemaphoreType.DMA((nf,)),
         ],
         compiler_params=pltpu.CompilerParams(
-            collective_id=1, has_side_effects=True, vmem_limit_bytes=16 * 2**20
+            collective_id=1, has_side_effects=True, vmem_limit_bytes=48 * 2**20
         ),
-    )(*blocks)
+    )(q_tail, b_block, k_block, far, master, basis, direction)
     return [out.reshape(-1, out.shape[-1]) for out in outs]
 
 
@@ -344,14 +437,17 @@
     block_branch = own_block(branch_basis)
     own_branch = block_branch.astype(jnp.float32)
     lanes = -key_local % 128
-    low, branch_low, squares = reduced(
+    early = rows_in // 32 * 20
+    low, branch_low, squares, far = reduced(
         n_rows,
         n_cols,
+        early,
         normed_inputs,
         query_upstream,
         jnp.pad(key_upstream, ((0, 0), (0, lanes))),
         head_outputs,
         branch_upstream,
+        query_master,
         own_block(query_basis),
         own_block(key_basis),
         block_branch,
@@ -381,9 +477,13 @@
     query_copy, branch_copy, key_copy = gathered_rows(
         n_rows,
         n_cols,
-        query_updated.astype(jnp.bfloat16),
+        query_updated[early:].astype(jnp.bfloat16),
         branch_updated.astype(jnp.bfloat16),
         jnp.pad(key_updated, ((0, 0), (0, lanes))).astype(jnp.bfloat16),
+        far,
+        query_master,
+        query_basis,
+        q_dir,
     )
     key_copy = key_copy[:, :key_local]
     return (

time: 180 us -> 164 us (0.911); the launches traced: 177 us -> 163 us
  Pallas kernels: 152 us -> 137 us
  other arithmetic: 0.3 us -> 4.05 us
  local copies, waits for them, and re-layouts: 14.3 us -> 12.3 us
    pallas_call x1, Pallas kernels: 81 us -> 59.2 us  [gathered_rows(): pl.pallas_call(functools.partial(gather_kernel, nf, nt), out_shape=tuple(...]
    pallas_call x1, Pallas kernels: 70.8 us -> 77.5 us  [reduced(): pl.pallas_call(functools.partial(reduce_kernel, nf, nt), out_shape=(jax.S...]
    unnamed x45 -> x37, local copies, waits for them, and re-layouts: 12.8 us -> 7.71 us
    dynamic_slice x2, local copies, waits for them, and re-layouts: 1 us -> 3.26 us  [own_block(): return lax.dynamic_slice_in_dim(basis, col_index * features, features, 0)]
    div x0 -> x1, other arithmetic: none -> 1.95 us  [moments(): first_new / (jnp.sqrt(second_new) + ADAM_EPS)]
where the time goes in v3:
time: 164 us; the launch traced here: 163 us
  Pallas kernels  137 us (84%)
  local copies, waits for them, and re-layouts  12.3 us (8%)
  matrix products  8.42 us (5%)
  other arithmetic  4.05 us (2%)
    pallas_call x1, Pallas kernels, reduced(): pl.pallas_call(functools.partial(reduce_kernel, nf, nt), out_shape=(jax.S...  77.5 us
    pallas_call x1, Pallas kernels, gathered_rows(): pl.pallas_call(functools.partial(gather_kernel, nf, nt), out_shape=tuple(...  59.2 us
    unnamed x37, local copies, waits for them, and re-layouts  7.71 us

profile of v3, /device:TPU:0, one launch (start us, length us, event | category | flops | bytes accessed | tf_op | source)
XLA Modules:
  0.0 163.0 jit_solution(16009368587692755878)
XLA Ops:
  0.7 1.6 constant_dynamic-slice_fusion.2.qb_ref
  2.2 1.7 %constant_dynamic-slice_fusion = (bf16[512,128]{1,0:T(8,128)(2,1)}, bf16[512,128]{1,0:T(8,128)(2,1)}) fusion(bf16[4096,128]{1,0:T(8,128)(2,1)} %param.27, s32[]{:T(128)S(6)} %select_n.10, bf16[4096,128]{1,0:T(8,128)(2,1)} %param.26), kind=kLoop, calls=%fused_computation.32 | loop fusion | bytes 524292 | tf_op jit(solution)/shard_map/dynamic_slice | solution.py:435
  3.9 77.5 %shard_map.280 = (f32[128,640]{1,0:T(8,128)}, f32[2,4,128,128]{3,2,1,0:T(8,128)}, f32[8,128]{1,0:T(8,128)}, f32[4,640,512]{2,1,0:T(8,128)}) custom-call(bf16[1024,512]{1,0:T(8,128)(2,1)} %x_hbm.1, bf16[1024,512]{1,0:T(8,128)(2,1)} %qu_hbm.1, bf16[1024,128]{1,0:T(8,128)(2,1)} %ku_hbm.1, bf16[1024,512]{1,0:T(8,128)(2,1)} %h_hbm.1, bf16[1024,512]{1,0:T(8,128)(2,1)} %bu_hbm.1, ...), custom_call_target="tpu_custom_call" | custom-call | tf_op jit(solution)/shard_map/pallas_call | solution.py:264
  81.4 0.0 copy-start.8
  81.4 0.0 copy-start.9
  81.4 1.3 slice.13
  83.5 1.1 broadcast_multiply_fusion
  84.5 0.0 copy-done.15
  84.5 0.0 copy-done.16
  84.6 0.9 fusion.12
  85.4 0.0 copy-start.11
  85.4 0.0 copy-start.12
  85.5 0.0 copy-done.13
  85.5 0.0 copy-start.10
  85.5 2.0 %add_divide_fusion = (f32[128,512]{1,0:T(8,128)S(1)}, f32[128,512]{1,0:T(8,128)}, f32[128,512]{1,0:T(8,128)}) fusion(f32[128,640]{1,0:T(8,128)} %get-tuple-element.23, f32[]{:T(128)} %bitcast, f32[128,512]{1,0:T(8,128)S(1)} %copy-done.13, f32[128,512]{1,0:T(8,128)S(1)} %copy-done.14), kind=kLoop, calls=%fused_computation.18 | loop fusion | flops 655360 | bytes 1572868 | tf_op jit(solution)/shard_map/div | solution.py:21
  87.4 0.0 copy-done.9
  87.4 0.0 copy-start.1
  87.5 0.2 fusion
  87.6 0.0 copy-start.4
  87.6 0.0 copy-start.5
  87.6 0.0 copy-done.11
  87.7 0.0 copy-done.12
  87.7 0.0 copy-done.10
  87.7 2.8 %fusion.21 = (bf16[1024,128]{1,0:T(8,128)(2,1)S(1)}, f32[1024,128]{1,0:T(8,128)}, f32[1024,128]{1,0:T(8,128)}) fusion(f32[1024,128]{1,0:T(8,128)S(1)} %copy-done.10, f32[128,128]{1,0:T(8,128)S(1)} %get-tuple-element.72, f32[128,128]{1,0:T(8,128)S(1)} %get-tuple-element.73, bf16[4096,128]{1,0:T(8,128)(2,1)} %param.26, s32[]{:T(128)S(6)} %select_n.4), kind=kOutput, calls=%fused_computation.38 | convolution fusion | flops 201752576 | bytes 2228228 | tf_op jit(solution)/shard_map/dot_general | solution.py:472
  90.5 0.0 copy-done.1
  90.5 0.0 copy-start.7
  90.5 2.4 %multiply_subtract_fusion.1 = (f32[1024,512]{1,0:T(8,128)S(1)}, f32[1024,512]{1,0:T(8,128)}) fusion(f32[1024,512]{1,0:T(8,128)S(1)} %copy-done, f32[128,512]{1,0:T(8,128)S(1)} %get-tuple-element.33.dir_ref, bf16[4096,128]{1,0:T(8,128)(2,1)S(1)} %copy-done.1, s32[]{:T(128)S(6)} %select_n.4), kind=kOutput, calls=%fused_computation.1 | convolution fusion | flops 806354944 | bytes 6815748 | tf_op jit(solution)/shard_map/dot_general | solution.py:471
  93.0 3.2 %fusion.22 = (bf16[1024,512]{1,0:T(8,128)(2,1)S(1)}, f32[1024,512]{1,0:T(8,128)}, f32[1024,512]{1,0:T(8,128)}) fusion(f32[1024,512]{1,0:T(8,128)S(1)} %copy-done.6, bf16[512,128]{1,0:T(8,128)(2,1)S(1)} %copy-done.7, f32[1024,128]{1,0:T(8,128)S(1)} %get-tuple-element.74, f32[1024,128]{1,0:T(8,128)S(1)} %get-tuple-element.75), kind=kOutput, calls=%fused_computation.39 | convolution fusion | flops 807141376 | bytes 8519680 | tf_op jit(solution)/shard_map/dot_general | solution.py:473
  96.2 59.2 %shard_map.281 = (bf16[4,1024,512]{2,1,0:T(8,128)(2,1)}, bf16[4,1024,512]{2,1,0:T(8,128)(2,1)}, bf16[4,1024,128]{2,1,0:T(8,128)(2,1)S(1)}) custom-call(bf16[384,512]{1,0:T(8,128)(2,1)S(1)} %slice.29.q_ref, bf16[1024,512]{1,0:T(8,128)(2,1)S(1)} %get-tuple-element.31.b_ref, bf16[1024,128]{1,0:T(8,128)(2,1)S(1)} %get-tuple-element.29.k_ref, ...), custom_call_target="tpu_custom_call" | custom-call | tf_op jit(solution)/shard_map/pallas_call | solution.py:384
  155.4 4.6 %copy.35 = bf16[4096,512]{1,0:T(8,128)(2,1)} copy(bf16[4096,512]{1,0:T(8,128)(2,1)} %bitcast.13) | data formatting | bytes 8388608
  160.0 1.0 copy.36
  161.0 2.0 %copy.37 = bf16[4096,512]{1,0:T(8,128)(2,1)} copy(bf16[4096,512]{1,0:T(8,128)(2,1)S(1)} %bitcast.12) | data formatting | bytes 8388608
  (18 shorter events, 0.1 us)
Async XLA Ops:
  3.9 80.6 %copy-start.15 = (f32[128,128]{1,0:T(8,128)S(1)}, f32[128,128]{1,0:T(8,128)}, u32[]{:S(2)}) copy-start(f32[128,128]{1,0:T(8,128)} %param.31) | copy-start | bytes 196612
  3.9 80.6 %copy-start.16 = (f32[128,128]{1,0:T(8,128)S(1)}, f32[128,128]{1,0:T(8,128)}, u32[]{:S(2)}) copy-start(f32[128,128]{1,0:T(8,128)} %param.30) | copy-start | bytes 196612
  3.9 81.5 %copy-start.13 = (f32[128,512]{1,0:T(8,128)S(1)}, f32[128,512]{1,0:T(8,128)}, u32[]{:S(2)}) copy-start(f32[128,512]{1,0:T(8,128)} %param.29) | copy-start | bytes 786436
  3.9 81.5 %copy-start.14 = (f32[128,512]{1,0:T(8,128)S(1)}, f32[128,512]{1,0:T(8,128)}, u32[]{:S(2)}) copy-start(f32[128,512]{1,0:T(8,128)} %param.28) | copy-start | bytes 786436
  81.4 6.0 %copy-start.8 = (f32[1024,128]{1,0:T(8,128)S(1)}, f32[1024,128]{1,0:T(8,128)}, u32[]{:S(2)}) copy-start(f32[1024,128]{1,0:T(8,128)} %param.33) | copy-start | bytes 1572868
  81.4 6.0 %copy-start.9 = (f32[1024,128]{1,0:T(8,128)S(1)}, f32[1024,128]{1,0:T(8,128)}, u32[]{:S(2)}) copy-start(f32[1024,128]{1,0:T(8,128)} %param.32) | copy-start | bytes 1572868
  85.4 2.2 %copy-start.11 = (f32[128,128]{1,0:T(8,128)}, f32[128,128]{1,0:T(8,128)S(1)}, u32[]{:S(2)}) copy-start(f32[128,128]{1,0:T(8,128)S(1)} %get-tuple-element.73) | copy-start | bytes 196612
  85.4 2.2 %copy-start.12 = (f32[128,128]{1,0:T(8,128)}, f32[128,128]{1,0:T(8,128)S(1)}, u32[]{:S(2)}) copy-start(f32[128,128]{1,0:T(8,128)S(1)} %get-tuple-element.72) | copy-start | bytes 196612
  85.5 2.2 %copy-start.10 = (f32[1024,128]{1,0:T(8,128)S(1)}, f32[1024,128]{1,0:T(8,128)}, u32[]{:S(2)}) copy-start(f32[1024,128]{1,0:T(8,128)} %param.23) | copy-start | bytes 1572868
  87.4 3.1 %copy-start = (f32[1024,512]{1,0:T(8,128)S(1)}, f32[1024,512]{1,0:T(8,128)}, u32[]{:S(2)}) copy-start(f32[1024,512]{1,0:T(8,128)} %master_ref.3) | copy-start | bytes 6291460
  87.4 3.0 %copy-start.1 = (bf16[4096,128]{1,0:T(8,128)(2,1)S(1)}, bf16[4096,128]{1,0:T(8,128)(2,1)}, u32[]{:S(2)}) copy-start(bf16[4096,128]{1,0:T(8,128)(2,1)} %basis_ref.1) | copy-start | bytes 3145732
  87.6 5.4 %copy-start.4 = (f32[1024,128]{1,0:T(8,128)}, f32[1024,128]{1,0:T(8,128)S(1)}, u32[]{:S(2)}) copy-start(f32[1024,128]{1,0:T(8,128)S(1)} %get-tuple-element.75) | copy-start | bytes 1572868
  87.6 5.4 %copy-start.5 = (f32[1024,128]{1,0:T(8,128)}, f32[1024,128]{1,0:T(8,128)S(1)}, u32[]{:S(2)}) copy-start(f32[1024,128]{1,0:T(8,128)S(1)} %get-tuple-element.74) | copy-start | bytes 1572868
  90.5 2.5 %copy-start.6 = (f32[1024,512]{1,0:T(8,128)S(1)}, f32[1024,512]{1,0:T(8,128)}, u32[]{:S(2)}) copy-start(f32[1024,512]{1,0:T(8,128)} %param.24) | copy-start | bytes 6291460
  90.5 2.5 %copy-start.7 = (bf16[512,128]{1,0:T(8,128)(2,1)S(1)}, bf16[512,128]{1,0:T(8,128)(2,1)}, u32[]{:S(2)}) copy-start(bf16[512,128]{1,0:T(8,128)(2,1)} %get-tuple-element.44.bb_ref) | copy-start | bytes 393220
  92.9 3.3 %copy-start.3 = (f32[1024,512]{1,0:T(8,128)}, f32[1024,512]{1,0:T(8,128)S(1)}, u32[]{:S(2)}) copy-start(f32[1024,512]{1,0:T(8,128)S(1)} %get-tuple-element.64) | copy-start | bytes 6291460
  155.4 5.6 %copy-start.2 = (bf16[4,1024,512]{2,1,0:T(8,128)(2,1)S(1)}, bf16[4,1024,512]{2,1,0:T(8,128)(2,1)}, u32[]{:S(2)}) copy-start(bf16[4,1024,512]{2,1,0:T(8,128)(2,1)} %get-tuple-element.28) | copy-start | bytes 12582916
